TPU v7x, 32 devices: a whole 2x2x4 slice. The times are simulated.
32 devices in a mesh: ep: 4 (over y, x), tp: 8 (over z, core).
Axes of the slice: x: 2, y: 2, z: 4, core: 2. Of those that a mesh axis runs over, the one named last changes fastest.
Arguments:
- stream: bfloat16 [64, 2048], P('ep'), may hold values from -6 to 6
- norm_gain_attn: float32 [2048], replicated, may hold values from 0.1 to 1.9
- w_query: bfloat16 [2048, 2048], P('ep', 'tp'), may hold values from -0.125 to 0.125
- w_key: bfloat16 [2048, 2048], P('ep', 'tp'), may hold values from -0.125 to 0.125
- w_value: bfloat16 [2048, 2048], P('ep', 'tp'), may hold values from -0.125 to 0.125
- w_forget: bfloat16 [2048, 16], replicated, may hold values from -0.125 to 0.125
- forget_bias: float32 [16], replicated, may hold values from -2 to 2
- key_cache: bfloat16 [64, 1024, 2048], P('ep', None, 'tp'), may hold values from -1500 to 1500
- value_cache: bfloat16 [64, 1024, 2048], P('ep', None, 'tp'), may hold values from -6 to 6
- gate_cache: float32 [64, 16, 1024], P('ep', 'tp'), may hold values from -1024 to 0, as said below
- lengths: int32 [64], P('ep'), may hold values from 128 to 1024
- w_output: bfloat16 [2048, 2048], P('tp'), may hold values from -0.125 to 0.125
- norm_gain_ffn: float32 [2048], replicated, may hold values from 0.1 to 1.9
- routes: int32 [64, 2], replicated, may hold values from 0 to 3, all different within a row; in each aligned block of 16 rows (0 to 15, 16 to 31, ...) at most 16 rows name the same one
- route_weights: float32 [64, 2], replicated, may hold values from 0.2 to 1
- w_expert_gate: bfloat16 [4, 2048, 5632], P('ep', None, 'tp'), may hold values from -0.125 to 0.125
- w_expert_up: bfloat16 [4, 2048, 5632], P('ep', None, 'tp'), may hold values from -0.125 to 0.125
- expert_down_weight: bfloat16 [4, 5632, 2048], P('ep', 'tp'), may hold values from -0.078125 to 0.078125
Outputs:
- result: bfloat16 [64, 2048], P('ep', 'tp')
Inputs may be any that keep to these rules, and one draw needn't show every extreme that they name: `gate_cache`: never rises along positions. `routes`: in the rows of one index of ep no expert is named by more than 16 rows, and in some such block one is named by exactly 16.
All inputs are finite; a program needn't handle non-finite values.
Results may differ from a plain program's by a relative error of at most 0.014.
Values may be sent and summed in bfloat16 or wider, within the bound.
A program may use at most 64 MiB of HBM per device.

v0:
```python
import functools

import jax
import jax.numpy as jnp
from jax import lax
from jax.experimental import pallas as pl
from jax.experimental.pallas import tpu as pltpu
from jax.sharding import PartitionSpec as P

F32 = jnp.float32
BF16 = jnp.bfloat16
DOWN_GROUPS = 4


def rms_norm(values, gain):
    floats = values.astype(F32)
    scaled = floats * lax.rsqrt(jnp.mean(floats * floats, axis=-1, keepdims=True) + 1e-06)
    return (scaled * gain).astype(BF16)


def matmul(a, b):
    return jnp.dot(a, b, preferred_element_type=F32)


def matmul_t(a, b):
    return lax.dot_general(a, b, (((1,), (1,)), ((), ())), preferred_element_type=F32)


def flip(index, bits):
    moved, bit = index, 1
    while bit <= bits:
        if bits & bit:
            moved = moved + bit - 2 * bit * lax.rem(lax.div(index, bit), 2)
        bit *= 2
    return moved


def layer_kernel(
    n_ep,
    n_tp,
    heads,
    stream,
    gain_attn,
    w_forget,
    forget_bias,
    gates,
    lengths,
    gain_ffn,
    routes,
    route_weights,
    wq_hbm,
    wk_hbm,
    wv_hbm,
    keys_hbm,
    values_hbm,
    wo_hbm,
    wg_hbm,
    wu_hbm,
    wd_hbm,
    out,
    wqkv,
    keys,
    values,
    wo,
    wg,
    wu,
    wd,
    a2a_send,
    a2a_recv,
    part_send,
    part_recv,
    gate_rows,
    scores,
    weights,
    rs_send,
    rs_recv,
    mix,
    dn_send,
    dn_recv,
    fs_send,
    fs_recv,
    w_sem,
    k_sem,
    v_sem,
    a2a_ss,
    a2a_rs,
    part_ss,
    part_rs,
    rs_ss,
    rs_rs,
    ag_ss,
    ag_rs,
    fw_ss,
    fw_rs,
    ps_ss,
    ps_rs,
    dn_ss,
    dn_rs,
    fs_ss,
    fs_rs,
):
    my_ep = lax.axis_index("ep")
    my_tp = lax.axis_index("tp")
    seqs, width = stream.shape
    depth = wq_hbm.shape[0]
    cols = wq_hbm.shape[1]
    cache = keys.shape[1]
    head_dim = cols // heads
    slice_w = out.shape[1]
    rows = heads * seqs
    tokens = n_ep * seqs

    def ep_at(k):
        return flip(my_ep, k)

    def tp_at(d):
        return flip(my_tp, d)

    def to_ep(src, dst, ss, rs, k):
        return pltpu.make_async_remote_copy(
            src_ref=src,
            dst_ref=dst,
            send_sem=ss,
            recv_sem=rs,
            device_id={"ep": ep_at(k)},
            device_id_type=pl.DeviceIdType.MESH,
        )

    def to_tp(src, dst, ss, rs, d):
        return pltpu.make_async_remote_copy(
            src_ref=src,
            dst_ref=dst,
            send_sem=ss,
            recv_sem=rs,
            device_id={"tp": tp_at(d)},
            device_id_type=pl.DeviceIdType.MESH,
        )

    barrier = pltpu.get_barrier_semaphore()
    for k in range(1, n_ep):
        pl.semaphore_signal(
            barrier, inc=1, device_id={"ep": ep_at(k)}, device_id_type=pl.DeviceIdType.MESH
        )
    for d in range(1, n_tp):
        pl.semaphore_signal(
            barrier, inc=1, device_id={"tp": tp_at(d)}, device_id_type=pl.DeviceIdType.MESH
        )

    loads = [
        pltpu.make_async_copy(src, dst, w_sem.at[i])
        for i, (src, dst) in enumerate(
            (
                (wq_hbm, wqkv.at[0]),
                (wk_hbm, wqkv.at[1]),
                (wv_hbm, wqkv.at[2]),
                (wo_hbm, wo),
                (wg_hbm.at[0], wg),
                (wu_hbm.at[0], wu),
                (wd_hbm.at[0], wd),
            )
        )
    ]

    def key_load(s):
        return pltpu.make_async_copy(keys_hbm.at[s], keys.at[s], k_sem.at[s])

    def value_load(s):
        return pltpu.make_async_copy(values_hbm.at[s], values.at[s], v_sem.at[s])

    for load in loads[:3]:
        load.start()

    @pl.loop(0, seqs)
    def _(s):
        key_load(s).start()

    @pl.loop(0, seqs)
    def _(s):
        value_load(s).start()

    for load in loads[3:]:
        load.start()

    normed = rms_norm(stream[...], gain_attn[...])
    for e in range(n_ep):
        a2a_send[e] = normed[:, e * depth : (e + 1) * depth]
    forget_all = matmul_t(normed, w_forget[...]) + forget_bias[...]
    forget_all = -(jnp.maximum(-forget_all, 0.0) + jnp.log1p(jnp.exp(-jnp.abs(forget_all))))

    pl.semaphore_wait(barrier, n_ep + n_tp - 2)

    sent = []
    a2a = []
    for k in range(1, n_ep):
        copy = to_ep(a2a_send.at[ep_at(k)], a2a_recv.at[my_ep], a2a_ss.at[k], a2a_rs.at[k], k)
        copy.start()
        a2a.append(copy)
    sent += a2a
    a2a_recv[my_ep] = a2a_send[my_ep]

    head_lane = lax.broadcasted_iota(jnp.int32, forget_all.shape, 1)
    forget_new = jnp.concatenate(
        [
            jnp.sum(
                jnp.where(head_lane == my_tp * heads + h, forget_all, 0.0), axis=1, keepdims=True
            )
            for h in range(heads)
        ],
        axis=0,
    )
    for h in range(heads):
        for s in range(seqs):
            r = h * seqs + s
            gate_rows[r : r + 1, :] = gates[s, h : h + 1, :]
    row_seq = lax.rem(lax.broadcasted_iota(jnp.int32, (rows, 1), 0), seqs)
    live_count = jnp.zeros((rows, 1), jnp.int32)
    for s in range(seqs):
        live_count = jnp.where(row_seq == s, lengths[s], live_count)
    position = lax.broadcasted_iota(jnp.int32, (rows, cache), 1)
    last_gate = jnp.sum(
        jnp.where(position == live_count - 1, gate_rows[...], 0.0), axis=1, keepdims=True
    )

    for load in loads[:3]:
        load.wait()
    for copy in a2a:
        copy.wait_recv()
    block = a2a_recv[...].reshape(tokens, depth)
    parts = []
    for i in range(3):
        product = matmul(block, wqkv[i])
        for e in range(n_ep):
            part_send[i, e] = product[e * seqs : (e + 1) * seqs]
        step = []
        for k in reversed(range(1, n_ep)):
            copy = to_ep(
                part_send.at[i, ep_at(k)],
                part_recv.at[i, my_ep],
                part_ss.at[i, k],
                part_rs.at[i, k],
                k,
            )
            copy.start()
            step.append(copy)
        parts.append(step)
        sent += step
        part_recv[i, my_ep] = part_send[i, my_ep]

    def projected(i):
        for copy in parts[i]:
            copy.wait_recv()
        total = part_recv[i, 0]
        for e in range(1, n_ep):
            total = total + part_recv[i, e]
        return total.astype(BF16).astype(F32)

    query = projected(0)
    scale = head_dim ** (-0.5)
    lane_head = lax.broadcasted_iota(jnp.int32, (seqs, cols), 1) // head_dim
    spread = jnp.concatenate(
        [jnp.where(lane_head == h, query, 0.0) for h in range(heads)], axis=0
    )
    spread = spread.astype(BF16)

    @pl.loop(0, seqs)
    def _(s):
        key_load(s).wait()

    for s in range(seqs):
        found = matmul_t(spread, keys[s])
        for h in range(heads):
            r = h * seqs + s
            scores[r : r + 1, :] = found[r : r + 1]
    key_new = projected(1)
    value_new = projected(2)
    own_score = (
        jnp.concatenate(
            [
                jnp.sum(
                    jnp.where(lane_head == h, query * key_new, 0.0), axis=1, keepdims=True
                )
                for h in range(heads)
            ],
            axis=0,
        )
        * scale
    )
    live = position < live_count
    full = scores[...] * scale + forget_new + last_gate - gate_rows[...]
    full = jnp.where(live, full, -1e30)
    largest = jnp.maximum(jnp.max(full, axis=1, keepdims=True), own_score)
    past = jnp.exp(full - largest)
    own_term = jnp.exp(own_score - largest)
    total = jnp.sum(past, axis=1, keepdims=True) + own_term
    weights[...] = (past / total).astype(BF16)
    own_weight = (own_term / total).astype(BF16).astype(F32)

    @pl.loop(0, seqs)
    def _(s):
        value_load(s).wait()

    gathered = jnp.zeros((rows, cols), F32)
    past_weights = weights[...]
    for s in range(seqs):
        gathered = jnp.where(row_seq == s, matmul(past_weights, values[s]), gathered)
    attended = jnp.zeros((seqs, cols), F32)
    for h in range(heads):
        part = slice(h * seqs, (h + 1) * seqs)
        attended = jnp.where(
            lane_head == h, gathered[part] + own_weight[part] * value_new, attended
        )
    attended = attended.astype(BF16)

    loads[3].wait()
    reduced = []
    for d in reversed(range(n_tp)):
        j = tp_at(d)
        at = pl.ds(pl.multiple_of(j * slice_w, slice_w), slice_w)
        rs_send[d] = matmul(attended, wo[:, at]).astype(BF16)
        if d:
            copy = to_tp(rs_send.at[d], rs_recv.at[d], rs_ss.at[d], rs_rs.at[d], d)
            copy.start()
            reduced.append(copy)
    sent += reduced
    head_total = rs_send[0].astype(F32)
    for d in range(1, n_tp):
        reduced[-d].wait_recv()
        head_total = head_total + rs_recv[d].astype(F32)
    own_at = pl.ds(pl.multiple_of(my_tp * slice_w, slice_w), slice_w)
    own_stream = (stream[:, own_at].astype(F32) + head_total).astype(BF16)
    core, level, levels = lax.rem(my_tp, 2), lax.div(my_tp, 2), n_tp // 2
    mix[core, my_ep, level] = own_stream

    gather = []
    for d in reversed(range(1, levels)):
        here = mix.at[core, my_ep, level]
        copy = to_tp(here, here, ag_ss.at[d], ag_rs.at[d], 2 * d)
        copy.start()
        gather.append(copy)
    sent += gather
    forward = [[] for _ in range(n_ep)]
    for d in range(levels):
        if d:
            gather[-d].wait_recv()
        here = mix.at[core, my_ep, flip(level, d)]
        for k in reversed(range(1, n_ep)):
            copy = to_ep(here, here, fw_ss.at[d, k], fw_rs.at[d, k], k)
            copy.start()
            forward[k].append(copy)
            sent.append(copy)
    passed = []
    for k in range(n_ep):
        for copy in forward[k]:
            copy.wait_recv()
        here = mix.at[core, ep_at(k)]
        copy = to_tp(here, here, ps_ss.at[k], ps_rs.at[k], 1)
        copy.start()
        passed.append(copy)
    sent += passed

    share = jnp.sum(
        jnp.where(routes[...] == my_ep, route_weights[...], 0.0), axis=0, keepdims=True
    )
    square = (tokens, tokens)
    diagonal = lax.broadcasted_iota(jnp.int32, square, 0) == lax.broadcasted_iota(
        jnp.int32, square, 1
    )
    coefficient = jnp.sum(jnp.where(diagonal, share, 0.0), axis=1, keepdims=True)
    for load in loads[4:]:
        load.wait()
    for copy in passed:
        copy.wait_recv()
    mixed = jnp.concatenate(
        [
            jnp.concatenate([mix[t % 2, e, t // 2] for t in range(n_tp)], axis=1) for e in range(n_ep)
        ],
        axis=0,
    )
    normed_ffn = rms_norm(mixed, gain_ffn[...])
    gate = matmul_t(normed_ffn, wg[...])
    up = matmul_t(normed_ffn, wu[...])
    hidden = (gate / (1.0 + jnp.exp(-gate)) * up).astype(BF16)

    down = []
    size = n_tp // DOWN_GROUPS
    for g in reversed(range(DOWN_GROUPS)):
        for d in reversed(range(g * size, (g + 1) * size)):
            at = pl.ds(pl.multiple_of(tp_at(d) * slice_w, slice_w), slice_w)
            product = (matmul(hidden, wd[:, at]) * coefficient).astype(BF16)
            for e in range(n_ep):
                dn_send[e, d] = product[e * seqs : (e + 1) * seqs]
        step = []
        group = pl.ds(g * size, size)
        for k in range(1, n_ep):
            copy = to_ep(
                dn_send.at[ep_at(k), group],
                dn_recv.at[k, group],
                dn_ss.at[g, k],
                dn_rs.at[g, k],
                k,
            )
            copy.start()
            step.append(copy)
        down.append(step)
        sent += step
    final = []
    for d in reversed(range(n_tp)):
        if d % size == size - 1:
            for copy in down[DOWN_GROUPS - 1 - d // size]:
                copy.wait_recv()
        summed = dn_send[my_ep, d].astype(F32)
        for k in range(1, n_ep):
            summed = summed + dn_recv[k, d].astype(F32)
        if d:
            fs_send[d] = summed.astype(BF16)
            copy = to_tp(fs_send.at[d], fs_recv.at[d], fs_ss.at[d], fs_rs.at[d], d)
            copy.start()
            final.append(copy)
    sent += final
    combined = summed
    for d in range(1, n_tp):
        final[-d].wait_recv()
        combined = combined + fs_recv[d].astype(F32)
    out[...] = (own_stream.astype(F32) + combined).astype(BF16)
    for copy in sent:
        copy.wait_send()


def shards(
    stream,
    norm_gain_attn,
    w_query,
    w_key,
    w_value,
    w_forget,
    forget_bias,
    key_cache,
    value_cache,
    gate_cache,
    lengths,
    w_output,
    norm_gain_ffn,
    routes,
    route_weights,
    w_expert_gate,
    w_expert_up,
    expert_down_weight,
):
    n_ep = lax.axis_size("ep")
    n_tp = lax.axis_size("tp")
    seqs, width = stream.shape
    heads = gate_cache.shape[1]
    cache = key_cache.shape[1]
    depth, cols = w_query.shape
    hidden = w_expert_gate.shape[2]
    slice_w = width // n_tp
    rows = heads * seqs
    vmem = pl.BlockSpec(memory_space=pltpu.VMEM)
    smem = pl.BlockSpec(memory_space=pltpu.SMEM)
    hbm = pl.BlockSpec(memory_space=pl.ANY)
    dma = pltpu.SemaphoreType.DMA
    return pl.pallas_call(
        functools.partial(layer_kernel, n_ep, n_tp, heads),
        out_shape=jax.ShapeDtypeStruct((seqs, slice_w), BF16),
        in_specs=[vmem] * 5 + [smem] + [vmem] * 3 + [hbm] * 9,
        out_specs=vmem,
        scratch_shapes=[
            pltpu.VMEM((3, depth, cols), BF16),
            pltpu.VMEM((seqs, cache, cols), BF16),
            pltpu.VMEM((seqs, cache, cols), BF16),
            pltpu.VMEM((cols, width), BF16),
            pltpu.VMEM((hidden, width), BF16),
            pltpu.VMEM((hidden, width), BF16),
            pltpu.VMEM((hidden, width), BF16),
            pltpu.VMEM((n_ep, seqs, depth), BF16),
            pltpu.VMEM((n_ep, seqs, depth), BF16),
            pltpu.VMEM((3, n_ep, seqs, cols), F32),
            pltpu.VMEM((3, n_ep, seqs, cols), F32),
            pltpu.VMEM((rows, cache), F32),
            pltpu.VMEM((rows, cache), F32),
            pltpu.VMEM((rows, cache), BF16),
            pltpu.VMEM((n_tp, seqs, slice_w), BF16),
            pltpu.VMEM((n_tp, seqs, slice_w), BF16),
            pltpu.VMEM((2, n_ep, n_tp // 2, seqs, slice_w), BF16),
            pltpu.VMEM((n_ep, n_tp, seqs, slice_w), BF16),
            pltpu.VMEM((n_ep, n_tp, seqs, slice_w), BF16),
            pltpu.VMEM((n_tp, seqs, slice_w), BF16),
            pltpu.VMEM((n_tp, seqs, slice_w), BF16),
            dma((7,)),
            dma((seqs,)),
            dma((seqs,)),
            dma((n_ep,)),
            dma((n_ep,)),
            dma((3, n_ep)),
            dma((3, n_ep)),
            dma((n_tp,)),
            dma((n_tp,)),
            dma((n_tp,)),
            dma((n_tp,)),
            dma((n_tp // 2, n_ep)),
            dma((n_tp // 2, n_ep)),
            dma((n_ep,)),
            dma((n_ep,)),
            dma((DOWN_GROUPS, n_ep)),
            dma((DOWN_GROUPS, n_ep)),
            dma((n_tp,)),
            dma((n_tp,)),
        ],
        compiler_params=pltpu.CompilerParams(
            collective_id=0, has_side_effects=True, vmem_limit_bytes=56 * 1024 * 1024
        ),
    )(
        stream,
        norm_gain_attn[None, :],
        w_forget.T,
        forget_bias[None, :],
        gate_cache,
        lengths,
        norm_gain_ffn[None, :],
        routes.T,
        route_weights.T,
        w_query,
        w_key,
        w_value,
        key_cache,
        value_cache,
        w_output,
        jnp.swapaxes(w_expert_gate, 1, 2),
        jnp.swapaxes(w_expert_up, 1, 2),
        expert_down_weight,
    )


def solution(mesh):
    placed = (
        P("ep", None),
        P(),
        P("ep", "tp"),
        P("ep", "tp"),
        P("ep", "tp"),
        P(),
        P(),
        P("ep", None, "tp"),
        P("ep", None, "tp"),
        P("ep", "tp", None),
        P("ep"),
        P("tp", None),
        P(),
        P(),
        P(),
        P("ep", None, "tp"),
        P("ep", None, "tp"),
        P("ep", "tp", None),
    )
    return jax.shard_map(
        shards, mesh=mesh, in_specs=placed, out_specs=P("ep", "tp"), check_vma=False
    )
```

profile of v0, /device:TPU:0, one launch (start us, length us, event | category | flops | bytes accessed | tf_op | source)
XLA Modules:
  0.0 42.1 jit_solution(15198827960503242464)
XLA Ops:
  0.0 40.8 %shard_map.172 = bf16[16,256]{1,0:T(8,128)(2,1)} custom-call(bf16[16,2048]{1,0:T(8,128)(2,1)} %stream.1, f32[1,2048]{1,0:T(1,128)} %bitcast.11, bf16[16,2048]{1,0:T(8,128)(2,1)} %bitcast.10, f32[1,16]{1,0:T(1,128)} %bitcast.15, f32[16,2,1024]{2,1,0:T(2,128)} %gates.1, s32[16]{0:T(128)} %lengths.1, f32[1,2048]{1,0:T(1,128)} %bitcast.12, s32[2,64]{1,0:T(2,128)} %bitcast.13, ...), custom_call_target="tpu_custom_call" | custom-call | tf_op jit(solution)/shard_map/pallas_call | solution.py:462
  40.8 1.3 %copy.20 = bf16[16,256]{1,0:T(8,128)(2,1)} copy(bf16[16,256]{1,0:T(8,128)(2,1)} %shard_map.172) | data formatting | bytes 16384
where the time goes:
time: 42.3 us; the launch traced here: 42.1 us
  Pallas kernels  40.8 us (96%)
  local copies, waits for them, and re-layouts  1.3 us (3%)
    pallas_call x1, Pallas kernels, shards(): pl.pallas_call(functools.partial(layer_kernel, n_ep, n_tp, heads), out_sh...  40.8 us
    unnamed x1, local copies, waits for them, and re-layouts  1.3 us

commit v1 on v0

v1 whole, which is shorter than its diff:
```python
import functools

import jax
import jax.numpy as jnp
from jax import lax
from jax.experimental import pallas as pl
from jax.experimental.pallas import tpu as pltpu
from jax.sharding import PartitionSpec as P

F32 = jnp.float32
BF16 = jnp.bfloat16
DOWN_GROUPS = 4
SEQ_GROUPS = 2
CACHE_LOADS = 4
LANES = 128


def inverse_rms(floats):
    return lax.rsqrt(jnp.mean(floats * floats, axis=-1, keepdims=True) + 1e-06)


def matmul(a, b):
    return jnp.dot(a, b, preferred_element_type=F32)


def matmul_t(a, b):
    return lax.dot_general(a, b, (((1,), (1,)), ((), ())), preferred_element_type=F32)


def flip(index, bits):
    moved, bit = index, 1
    while bit <= bits:
        if bits & bit:
            moved = moved + bit - 2 * bit * lax.rem(lax.div(index, bit), 2)
        bit *= 2
    return moved


def layer_kernel(
    n_ep,
    n_tp,
    heads,
    stream_hbm,
    gain_attn_hbm,
    w_forget_hbm,
    forget_bias_hbm,
    gates_hbm,
    lengths_hbm,
    gain_ffn_hbm,
    routes_hbm,
    route_weights_hbm,
    wq_hbm,
    wk_hbm,
    wv_hbm,
    keys_hbm,
    values_hbm,
    wo_hbm,
    wg_hbm,
    wu_hbm,
    wd_hbm,
    out,
    stream,
    gain_attn,
    w_forget,
    forget_bias,
    gates,
    lengths,
    gain_ffn,
    routes,
    route_weights,
    wqkv,
    keys,
    keys_t,
    values,
    wo,
    wg,
    wu,
    wd,
    wg_t,
    wu_t,
    a2a_send,
    a2a_recv,
    part_send,
    part_recv,
    gate_rows,
    pair_send,
    pair_recv,
    own_part,
    zs_send,
    zs_recv,
    mix,
    dn_send,
    dn_recv,
    fs_send,
    fs_recv,
    small_sem,
    w_sem,
    k_sem,
    v_sem,
    a2a_ss,
    a2a_rs,
    part_ss,
    part_rs,
    pair_ss,
    pair_rs,
    zs_ss,
    zs_rs,
    mix_ss,
    mix_rs,
    dn_ss,
    dn_rs,
    fs_ss,
    fs_rs,
):
    my_ep = lax.axis_index("ep")
    my_tp = lax.axis_index("tp")
    seqs, width = stream.shape
    depth = wq_hbm.shape[0]
    cols = wq_hbm.shape[1]
    cache = keys.shape[1]
    head_dim = cols // heads
    slice_w = out.shape[1]
    hidden_w = wg_hbm.shape[1]
    tokens = n_ep * seqs
    levels = n_tp // 2
    half_w = levels * slice_w
    core, level = lax.rem(my_tp, 2), lax.div(my_tp, 2)
    sg = seqs // SEQ_GROUPS
    grows = heads * sg
    rows = SEQ_GROUPS * grows

    def ep_at(k):
        return flip(my_ep, k)

    def tp_at(d):
        return flip(my_tp, d)

    def remote(src, dst, ss, rs, device):
        return pltpu.make_async_remote_copy(
            src_ref=src,
            dst_ref=dst,
            send_sem=ss,
            recv_sem=rs,
            device_id=device,
            device_id_type=pl.DeviceIdType.MESH,
        )

    barrier = pltpu.get_barrier_semaphore()
    for c in range(2):
        for k in range(1, n_ep):
            pl.semaphore_signal(
                barrier,
                inc=1,
                device_id={"ep": ep_at(k), "tp": tp_at(c)},
                device_id_type=pl.DeviceIdType.MESH,
            )
    for d in range(1, n_tp):
        pl.semaphore_signal(
            barrier, inc=1, device_id={"tp": tp_at(d)}, device_id_type=pl.DeviceIdType.MESH
        )

    small = [
        pltpu.make_async_copy(src, dst, small_sem.at[i])
        for i, (src, dst) in enumerate(
            (
                (stream_hbm, stream),
                (gain_attn_hbm, gain_attn),
                (w_forget_hbm, w_forget),
                (forget_bias_hbm, forget_bias),
                (gates_hbm, gates),
                (lengths_hbm, lengths),
                (gain_ffn_hbm, gain_ffn),
                (routes_hbm, routes),
                (route_weights_hbm, route_weights),
            )
        )
    ]
    loads = [
        pltpu.make_async_copy(src, dst, w_sem.at[i])
        for i, (src, dst) in enumerate(
            (
                (wq_hbm, wqkv.at[0]),
                (wk_hbm, wqkv.at[1]),
                (wv_hbm, wqkv.at[2]),
                (wo_hbm, wo),
                (wg_hbm.at[0], wg.at[pl.ds(0, hidden_w)]),
                (wu_hbm.at[0], wu.at[pl.ds(0, hidden_w)]),
                (wd_hbm.at[0], wd.at[pl.ds(0, hidden_w)]),
            )
        )
    ]
    span = seqs // CACHE_LOADS
    key_loads = [
        pltpu.make_async_copy(
            keys_hbm.at[pl.ds(i * span, span)], keys.at[pl.ds(i * span, span)], k_sem.at[i]
        )
        for i in range(CACHE_LOADS)
    ]
    value_loads = [
        pltpu.make_async_copy(
            values_hbm.at[pl.ds(i * span, span)], values.at[pl.ds(i * span, span)], v_sem.at[i]
        )
        for i in range(CACHE_LOADS)
    ]
    for load in small[:2] + loads[:3] + small[2:]:
        load.start()
    for load in key_loads + value_loads + loads[3:]:
        load.start(priority=1)

    spare = wg.shape[0] - hidden_w
    if spare:
        for w in (wg, wu, wd):
            w[hidden_w:, :] = jnp.zeros((spare, width), BF16)

    small[0].wait()
    small[1].wait()
    floats = stream[...].astype(F32)
    normed = (floats * inverse_rms(floats) * gain_attn[...]).astype(BF16)
    for e in range(n_ep):
        a2a_send[e] = normed[:, e * depth : (e + 1) * depth]

    pl.semaphore_wait(barrier, 2 * (n_ep - 1) + n_tp - 1)

    sent = []
    a2a = []
    for k in reversed(range(1, n_ep)):
        copy = remote(
            a2a_send.at[ep_at(k)], a2a_recv.at[my_ep], a2a_ss.at[k], a2a_rs.at[k], {"ep": ep_at(k)}
        )
        copy.start()
        a2a.append(copy)
    sent += a2a
    a2a_recv[my_ep] = a2a_send[my_ep]

    for load in small[2:]:
        load.wait()
    forget_all = matmul_t(normed, w_forget[...]) + forget_bias[...]
    forget_all = -(jnp.maximum(-forget_all, 0.0) + jnp.log1p(jnp.exp(-jnp.abs(forget_all))))
    head_lane = lax.broadcasted_iota(jnp.int32, (sg, forget_all.shape[1]), 1)
    forget_new = jnp.concatenate(
        [
            jnp.sum(
                jnp.where(
                    head_lane == my_tp * heads + h, forget_all[g * sg : (g + 1) * sg], 0.0
                ),
                axis=1,
                keepdims=True,
            )
            for g in range(SEQ_GROUPS)
            for h in range(heads)
        ],
        axis=0,
    )
    for g in range(SEQ_GROUPS):
        for h in range(heads):
            for s in range(sg):
                r = (g * heads + h) * sg + s
                gate_rows[r : r + 1, :] = gates[g * sg + s, h : h + 1, :]
    row = lax.broadcasted_iota(jnp.int32, (rows, seqs), 0)
    row_seq = row // grows * sg + row % sg
    length_f = lengths[...].astype(F32)
    live_count = jnp.sum(
        jnp.where(lax.broadcasted_iota(jnp.int32, (rows, seqs), 1) == row_seq, length_f, 0.0),
        axis=1,
        keepdims=True,
    ).astype(jnp.int32)
    position = lax.broadcasted_iota(jnp.int32, (rows, cache), 1)
    last_gate = jnp.sum(
        jnp.where(position == live_count - 1, gate_rows[...], 0.0), axis=1, keepdims=True
    )
    gate_rows[...] = jnp.where(
        position < live_count, forget_new + (last_gate - gate_rows[...]), -1e30
    )

    for load in loads[:3]:
        load.wait()
    for copy in a2a:
        copy.wait_recv()
    block = a2a_recv[...].reshape(tokens, depth)
    parts = []
    for i in range(3):
        product = matmul(block, wqkv[i])
        for e in range(n_ep):
            part_send[i, e] = product[e * seqs : (e + 1) * seqs]
        step = []
        for k in reversed(range(1, n_ep)):
            copy = remote(
                part_send.at[i, ep_at(k)],
                part_recv.at[i, my_ep],
                part_ss.at[i, k],
                part_rs.at[i, k],
                {"ep": ep_at(k)},
            )
            copy.start()
            step.append(copy)
        parts.append(step)
        sent += step
        part_recv[i, my_ep] = part_send[i, my_ep]

    for i in range(CACHE_LOADS):
        key_loads[i].wait()

        @pl.loop(i * span, (i + 1) * span)
        def _(s):
            keys_t[pl.ds(pl.multiple_of(s * cols, cols), cols), :] = keys[s].T

    def projected(i):
        for copy in parts[i]:
            copy.wait_recv()
        total = part_recv[i, 0]
        for e in range(1, n_ep):
            total = total + part_recv[i, e]
        return total.astype(BF16).astype(F32)

    scale = head_dim ** (-0.5)
    query = projected(0)
    lane_head = lax.broadcasted_iota(jnp.int32, (sg, cols), 1) // head_dim
    group_seq = lax.broadcasted_iota(jnp.int32, (grows, 1), 0) % sg

    def by_head(values_of):
        return jnp.concatenate(values_of, axis=0)

    def score(g):
        mine = query[g * sg : (g + 1) * sg]
        spread = by_head([jnp.where(lane_head == h, mine, 0.0) for h in range(heads)])
        lhs = jnp.concatenate(
            [jnp.where(group_seq == s, spread, 0.0).astype(BF16) for s in range(sg)], axis=1
        )
        return matmul(lhs, keys_t[g * sg * cols : (g + 1) * sg * cols, :])

    def finish_pair(g):
        pairs[g].wait_recv()
        zs_send[g] = (own_part[g] + pair_recv[g].astype(F32)).astype(BF16)
        step = []
        for d in reversed(range(1, levels)):
            copy = remote(
                zs_send.at[g], zs_recv.at[g, d], zs_ss.at[g, d], zs_rs.at[g, d], {"tp": tp_at(2 * d)}
            )
            copy.start()
            step.append(copy)
        zsum.append(step)
        sent.extend(step)

    pairs, zsum = [], []
    for g in range(SEQ_GROUPS):
        found = score(g)
        if g == 0:
            key_new = projected(1)
            value_new = projected(2)
        mine = slice(g * sg, (g + 1) * sg)
        own_score = (
            by_head(
                [
                    jnp.sum(
                        jnp.where(lane_head == h, query[mine] * key_new[mine], 0.0),
                        axis=1,
                        keepdims=True,
                    )
                    for h in range(heads)
                ]
            )
            * scale
        )
        full = found * scale + gate_rows[g * grows : (g + 1) * grows, :]
        largest = jnp.maximum(jnp.max(full, axis=1, keepdims=True), own_score)
        past = jnp.exp(full - largest)
        own_term = jnp.exp(own_score - largest)
        total = jnp.sum(past, axis=1, keepdims=True) + own_term
        past_weights = past / total
        own_weight = (own_term / total).astype(BF16).astype(F32)
        if g:
            finish_pair(g - 1)
        for i in range(CACHE_LOADS):
            if i * span // sg == g:
                value_loads[i].wait()
        gathered = jnp.zeros((grows, cols), F32)
        for s in range(sg):
            chosen = jnp.where(group_seq == s, past_weights, 0.0).astype(BF16)
            gathered = gathered + matmul(chosen, values[g * sg + s])
        attended = jnp.zeros((sg, cols), F32)
        for h in range(heads):
            part = slice(h * sg, (h + 1) * sg)
            attended = jnp.where(
                lane_head == h, gathered[part] + own_weight[part] * value_new[mine], attended
            )
        attended = attended.astype(BF16)
        if g == 0:
            loads[3].wait()

        def outward(c):
            return jnp.concatenate(
                [
                    matmul(
                        attended,
                        wo[:, pl.ds(pl.multiple_of((2 * t + c) * slice_w, slice_w), slice_w)],
                    )
                    for t in range(levels)
                ],
                axis=1,
            )

        pair_send[g] = outward(1 - core).astype(BF16)
        copy = remote(
            pair_send.at[g], pair_recv.at[g], pair_ss.at[g], pair_rs.at[g], {"tp": tp_at(1)}
        )
        copy.start()
        pairs.append(copy)
        sent.append(copy)
        own_part[g] = outward(core)
    finish_pair(SEQ_GROUPS - 1)

    stream_half = jnp.concatenate(
        [
            stream[:, pl.ds(pl.multiple_of((2 * t + core) * slice_w, slice_w), slice_w)]
            for t in range(levels)
        ],
        axis=1,
    ).astype(F32)

    def transposed(src, dst):
        @pl.loop(0, n_tp)
        def _(t):
            into = lax.rem(t, 2) * half_w + lax.div(t, 2) * slice_w
            dst[pl.ds(pl.multiple_of(into, slice_w), slice_w), :] = src[
                :, pl.ds(pl.multiple_of(t * slice_w, slice_w), slice_w)
            ].T

    mixes = []
    for g in range(SEQ_GROUPS):
        if g < 2:
            loads[4 + g].wait()
            transposed(*((wg, wg_t), (wu, wu_t))[g])
        total = stream_half[g * sg : (g + 1) * sg] + zs_send[g].astype(F32)
        for d in range(1, levels):
            zsum[g][-d].wait_recv()
            total = total + zs_recv[g, d].astype(F32)
        mix[core, my_ep, g] = total.astype(BF16)
        here = mix.at[core, my_ep, g]
        step = []
        for k in reversed(range(n_ep)):
            for c in range(2):
                if k or c:
                    copy = remote(
                        here,
                        here,
                        mix_ss.at[g, k, c],
                        mix_rs.at[g, k, c],
                        {"ep": ep_at(k), "tp": tp_at(c)},
                    )
                    copy.start()
                    step.append(copy)
        mixes += step
    sent += mixes

    share = jnp.sum(
        jnp.where(routes[...] == my_ep, route_weights[...], 0.0), axis=0, keepdims=True
    )
    square = (tokens, tokens)
    diagonal = lax.broadcasted_iota(jnp.int32, square, 0) == lax.broadcasted_iota(
        jnp.int32, square, 1
    )
    coefficient = jnp.sum(jnp.where(diagonal, share, 0.0), axis=1, keepdims=True)
    loads[6].wait()
    for copy in mixes:
        copy.wait_recv()
    halves = [mix[c].astype(F32).reshape(tokens, half_w) for c in range(2)]
    squares = sum(jnp.sum(half * half, axis=1, keepdims=True) for half in halves)
    inverse = lax.rsqrt(squares / width + 1e-06)
    normed_ffn = jnp.concatenate(
        [
            (
                halves[c]
                * inverse
                * jnp.concatenate(
                    [
                        gain_ffn[:, (2 * t + c) * slice_w : (2 * t + c + 1) * slice_w]
                        for t in range(levels)
                    ],
                    axis=1,
                )
            ).astype(BF16)
            for c in range(2)
        ],
        axis=1,
    )
    gate = matmul(normed_ffn, wg_t[...])
    up = matmul(normed_ffn, wu_t[...])
    hidden = (gate / (1.0 + jnp.exp(-gate)) * up).astype(BF16)

    down = []
    size = n_tp // DOWN_GROUPS
    for g in reversed(range(DOWN_GROUPS)):
        for d in reversed(range(g * size, (g + 1) * size)):
            at = pl.ds(pl.multiple_of(tp_at(d) * slice_w, slice_w), slice_w)
            product = (matmul(hidden, wd[:, at]) * coefficient).astype(BF16)
            for e in range(n_ep):
                dn_send[e, d] = product[e * seqs : (e + 1) * seqs]
        step = []
        group = pl.ds(g * size, size)
        for k in reversed(range(1, n_ep)):
            copy = remote(
                dn_send.at[ep_at(k), group],
                dn_recv.at[k, group],
                dn_ss.at[g, k],
                dn_rs.at[g, k],
                {"ep": ep_at(k)},
            )
            copy.start()
            step.append(copy)
        down.append(step)
        sent += step
    final = []
    for d in reversed(range(n_tp)):
        if d % size == size - 1:
            for copy in down[DOWN_GROUPS - 1 - d // size]:
                copy.wait_recv()
        summed = dn_send[my_ep, d].astype(F32)
        for k in range(1, n_ep):
            summed = summed + dn_recv[k, d].astype(F32)
        if d:
            fs_send[d] = summed.astype(BF16)
            copy = remote(fs_send.at[d], fs_recv.at[d], fs_ss.at[d], fs_rs.at[d], {"tp": tp_at(d)})
            copy.start()
            final.append(copy)
    sent += final
    combined = summed
    own_stream = mix[
        core, my_ep, :, :, pl.ds(pl.multiple_of(level * slice_w, slice_w), slice_w)
    ].astype(F32).reshape(seqs, slice_w)
    combined = own_stream + combined
    for d in range(1, n_tp):
        final[-d].wait_recv()
        combined = combined + fs_recv[d].astype(F32)
    out[...] = combined.astype(BF16)
    for copy in sent:
        copy.wait_send()


def shards(
    stream,
    norm_gain_attn,
    w_query,
    w_key,
    w_value,
    w_forget,
    forget_bias,
    key_cache,
    value_cache,
    gate_cache,
    lengths,
    w_output,
    norm_gain_ffn,
    routes,
    route_weights,
    w_expert_gate,
    w_expert_up,
    expert_down_weight,
):
    n_ep = lax.axis_size("ep")
    n_tp = lax.axis_size("tp")
    seqs, width = stream.shape
    heads = gate_cache.shape[1]
    cache = key_cache.shape[1]
    depth, cols = w_query.shape
    hidden = w_expert_gate.shape[2]
    padded = -(-hidden // LANES) * LANES
    slice_w = width // n_tp
    levels = n_tp // 2
    half_w = levels * slice_w
    rows = heads * seqs
    sg = seqs // SEQ_GROUPS
    vmem = pl.BlockSpec(memory_space=pltpu.VMEM)
    hbm = pl.BlockSpec(memory_space=pltpu.HBM)
    dma = pltpu.SemaphoreType.DMA
    small = (
        stream,
        norm_gain_attn[None, :],
        w_forget.T,
        forget_bias[None, :],
        gate_cache,
        lengths[None, :],
        norm_gain_ffn[None, :],
        routes.T,
        route_weights.T,
    )
    return pl.pallas_call(
        functools.partial(layer_kernel, n_ep, n_tp, heads),
        out_shape=jax.ShapeDtypeStruct((seqs, slice_w), BF16),
        in_specs=[hbm] * 18,
        out_specs=vmem,
        scratch_shapes=[pltpu.VMEM(array.shape, array.dtype) for array in small]
        + [
            pltpu.VMEM((3, depth, cols), BF16),
            pltpu.VMEM((seqs, cache, cols), BF16),
            pltpu.VMEM((seqs * cols, cache), BF16),
            pltpu.VMEM((seqs, cache, cols), BF16),
            pltpu.VMEM((cols, width), BF16),
            pltpu.VMEM((padded, width), BF16),
            pltpu.VMEM((padded, width), BF16),
            pltpu.VMEM((padded, width), BF16),
            pltpu.VMEM((width, padded), BF16),
            pltpu.VMEM((width, padded), BF16),
            pltpu.VMEM((n_ep, seqs, depth), BF16),
            pltpu.VMEM((n_ep, seqs, depth), BF16),
            pltpu.VMEM((3, n_ep, seqs, cols), F32),
            pltpu.VMEM((3, n_ep, seqs, cols), F32),
            pltpu.VMEM((rows, cache), F32),
            pltpu.VMEM((SEQ_GROUPS, sg, half_w), BF16),
            pltpu.VMEM((SEQ_GROUPS, sg, half_w), BF16),
            pltpu.VMEM((SEQ_GROUPS, sg, half_w), F32),
            pltpu.VMEM((SEQ_GROUPS, sg, half_w), BF16),
            pltpu.VMEM((SEQ_GROUPS, levels, sg, half_w), BF16),
            pltpu.VMEM((2, n_ep, SEQ_GROUPS, sg, half_w), BF16),
            pltpu.VMEM((n_ep, n_tp, seqs, slice_w), BF16),
            pltpu.VMEM((n_ep, n_tp, seqs, slice_w), BF16),
            pltpu.VMEM((n_tp, seqs, slice_w), BF16),
            pltpu.VMEM((n_tp, seqs, slice_w), BF16),
            dma((len(small),)),
            dma((7,)),
            dma((CACHE_LOADS,)),
            dma((CACHE_LOADS,)),
            dma((n_ep,)),
            dma((n_ep,)),
            dma((3, n_ep)),
            dma((3, n_ep)),
            dma((SEQ_GROUPS,)),
            dma((SEQ_GROUPS,)),
            dma((SEQ_GROUPS, levels)),
            dma((SEQ_GROUPS, levels)),
            dma((SEQ_GROUPS, n_ep, 2)),
            dma((SEQ_GROUPS, n_ep, 2)),
            dma((DOWN_GROUPS, n_ep)),
            dma((DOWN_GROUPS, n_ep)),
            dma((n_tp,)),
            dma((n_tp,)),
        ],
        compiler_params=pltpu.CompilerParams(
            collective_id=0, has_side_effects=True, vmem_limit_bytes=56 * 1024 * 1024
        ),
    )(
        *small,
        w_query,
        w_key,
        w_value,
        key_cache,
        value_cache,
        w_output,
        jnp.swapaxes(w_expert_gate, 1, 2),
        jnp.swapaxes(w_expert_up, 1, 2),
        expert_down_weight,
    )


def solution(mesh):
    placed = (
        P("ep", None),
        P(),
        P("ep", "tp"),
        P("ep", "tp"),
        P("ep", "tp"),
        P(),
        P(),
        P("ep", None, "tp"),
        P("ep", None, "tp"),
        P("ep", "tp", None),
        P("ep"),
        P("tp", None),
        P(),
        P(),
        P(),
        P("ep", None, "tp"),
        P("ep", None, "tp"),
        P("ep", "tp", None),
    )
    return jax.shard_map(
        shards, mesh=mesh, in_specs=placed, out_specs=P("ep", "tp"), check_vma=False
    )
```

time: 42.3 us -> 37 us (0.87)
  Pallas kernels: 40.8 us -> 35.5 us
    pallas_call x1, Pallas kernels: 40.8 us -> 35.5 us  [shards(): pl.pallas_call(functools.partial(layer_kernel, n_ep, n_tp, heads), out_sh...]
where the time goes in v1:
time: 37 us; the launch traced here: 36.8 us
  Pallas kernels  35.5 us (96%)
  local copies, waits for them, and re-layouts  1.3 us (4%)
    pallas_call x1, Pallas kernels, shards(): pl.pallas_call(functools.partial(layer_kernel, n_ep, n_tp, heads), out_sh...  35.5 us
    unnamed x1, local copies, waits for them, and re-layouts  1.3 us

profile of v1, /device:TPU:0, one launch (start us, length us, event | category | flops | bytes accessed | tf_op | source)
XLA Modules:
  0.0 36.8 jit_solution(10403929854579743633)
XLA Ops:
  0.0 35.5 %shard_map.172 = bf16[16,256]{1,0:T(8,128)(2,1)} custom-call(bf16[16,2048]{1,0:T(8,128)(2,1)} %stream_hbm.1, f32[1,2048]{1,0:T(1,128)} %bitcast.12, bf16[16,2048]{1,0:T(8,128)(2,1)} %bitcast.11, f32[1,16]{1,0:T(1,128)} %bitcast.16, f32[16,2,1024]{2,1,0:T(2,128)} %gates_hbm.1, s32[1,16]{1,0:T(1,128)} %bitcast.17, f32[1,2048]{1,0:T(1,128)} %bitcast.13, ...), custom_call_target="tpu_custom_call" | custom-call | tf_op jit(solution)/shard_map/pallas_call | solution.py:586
  35.5 1.3 %copy.20 = bf16[16,256]{1,0:T(8,128)(2,1)} copy(bf16[16,256]{1,0:T(8,128)(2,1)} %shard_map.172) | data formatting | bytes 16384

commit v2 on v1

--- a/solution.py
+++ b/solution.py
@@ -9,7 +9,6 @@
 
 F32 = jnp.float32
 BF16 = jnp.bfloat16
-DOWN_GROUPS = 4
 SEQ_GROUPS = 2
 CACHE_LOADS = 4
 LANES = 128
@@ -89,14 +88,16 @@
     zs_send,
     zs_recv,
     mix,
-    dn_send,
-    dn_recv,
+    dpair_send,
+    dpair_recv,
+    down_part,
     fs_send,
     fs_recv,
     small_sem,
     w_sem,
     k_sem,
     v_sem,
+    relay,
     a2a_ss,
     a2a_rs,
     part_ss,
@@ -107,8 +108,8 @@
     zs_rs,
     mix_ss,
     mix_rs,
-    dn_ss,
-    dn_rs,
+    dpair_ss,
+    dpair_rs,
     fs_ss,
     fs_rs,
 ):
@@ -145,19 +146,16 @@
             device_id_type=pl.DeviceIdType.MESH,
         )
 
+    def wait_all(ref, sem):
+        pltpu.make_async_copy(ref, ref, sem).wait()
+
+    others = pl.ds(1, n_ep - 1)
     barrier = pltpu.get_barrier_semaphore()
-    for c in range(2):
-        for k in range(1, n_ep):
-            pl.semaphore_signal(
-                barrier,
-                inc=1,
-                device_id={"ep": ep_at(k), "tp": tp_at(c)},
-                device_id_type=pl.DeviceIdType.MESH,
-            )
-    for d in range(1, n_tp):
-        pl.semaphore_signal(
-            barrier, inc=1, device_id={"tp": tp_at(d)}, device_id_type=pl.DeviceIdType.MESH
-        )
+    bits = [1 << b for b in range(levels.bit_length() - 1)]
+    met = [{"ep": ep_at(k)} for k in reversed(range(1, n_ep))]
+    met += [{"tp": tp_at(1)}] + [{"tp": tp_at(2 * b)} for b in bits]
+    for device in met:
+        pl.semaphore_signal(barrier, inc=1, device_id=device, device_id_type=pl.DeviceIdType.MESH)
 
     small = [
         pltpu.make_async_copy(src, dst, small_sem.at[i])
@@ -219,18 +217,19 @@
     for e in range(n_ep):
         a2a_send[e] = normed[:, e * depth : (e + 1) * depth]
 
-    pl.semaphore_wait(barrier, 2 * (n_ep - 1) + n_tp - 1)
-
-    sent = []
-    a2a = []
+    pl.semaphore_wait(barrier, len(met))
+
     for k in reversed(range(1, n_ep)):
-        copy = remote(
-            a2a_send.at[ep_at(k)], a2a_recv.at[my_ep], a2a_ss.at[k], a2a_rs.at[k], {"ep": ep_at(k)}
-        )
-        copy.start()
-        a2a.append(copy)
-    sent += a2a
-    a2a_recv[my_ep] = a2a_send[my_ep]
+        remote(a2a_send.at[ep_at(k)], a2a_recv.at[k], a2a_ss, a2a_rs, {"ep": ep_at(k)}).start()
+    a2a_recv[0] = a2a_send[my_ep]
+    for i, b in enumerate(bits[:-1]):
+        pl.semaphore_signal(
+            relay.at[i],
+            inc=1,
+            device_id={"tp": tp_at(2 * b)},
+            device_id_type=pl.DeviceIdType.MESH,
+        )
+        pl.semaphore_wait(relay.at[i], 1)
 
     for load in small[2:]:
         load.wait()
@@ -274,28 +273,16 @@
 
     for load in loads[:3]:
         load.wait()
-    for copy in a2a:
-        copy.wait_recv()
+    wait_all(a2a_recv.at[others], a2a_rs)
     block = a2a_recv[...].reshape(tokens, depth)
-    parts = []
     for i in range(3):
         product = matmul(block, wqkv[i])
-        for e in range(n_ep):
-            part_send[i, e] = product[e * seqs : (e + 1) * seqs]
-        step = []
         for k in reversed(range(1, n_ep)):
-            copy = remote(
-                part_send.at[i, ep_at(k)],
-                part_recv.at[i, my_ep],
-                part_ss.at[i, k],
-                part_rs.at[i, k],
-                {"ep": ep_at(k)},
-            )
-            copy.start()
-            step.append(copy)
-        parts.append(step)
-        sent += step
-        part_recv[i, my_ep] = part_send[i, my_ep]
+            part_send[i, k] = product[k * seqs : (k + 1) * seqs]
+            remote(
+                part_send.at[i, k], part_recv.at[i, k], part_ss, part_rs.at[i], {"ep": ep_at(k)}
+            ).start()
+        part_recv[i, 0] = product[:seqs]
 
     for i in range(CACHE_LOADS):
         key_loads[i].wait()
@@ -305,8 +292,7 @@
             keys_t[pl.ds(pl.multiple_of(s * cols, cols), cols), :] = keys[s].T
 
     def projected(i):
-        for copy in parts[i]:
-            copy.wait_recv()
+        wait_all(part_recv.at[i, others], part_rs.at[i])
         total = part_recv[i, 0]
         for e in range(1, n_ep):
             total = total + part_recv[i, e]
@@ -329,19 +315,13 @@
         return matmul(lhs, keys_t[g * sg * cols : (g + 1) * sg * cols, :])
 
     def finish_pair(g):
-        pairs[g].wait_recv()
+        wait_all(pair_recv.at[g], pair_rs.at[g])
         zs_send[g] = (own_part[g] + pair_recv[g].astype(F32)).astype(BF16)
-        step = []
         for d in reversed(range(1, levels)):
-            copy = remote(
-                zs_send.at[g], zs_recv.at[g, d], zs_ss.at[g, d], zs_rs.at[g, d], {"tp": tp_at(2 * d)}
-            )
-            copy.start()
-            step.append(copy)
-        zsum.append(step)
-        sent.extend(step)
-
-    pairs, zsum = [], []
+            remote(
+                zs_send.at[g], zs_recv.at[g, d], zs_ss, zs_rs.at[g], {"tp": tp_at(2 * d)}
+            ).start()
+
     for g in range(SEQ_GROUPS):
         found = score(g)
         if g == 0:
@@ -400,12 +380,9 @@
             )
 
         pair_send[g] = outward(1 - core).astype(BF16)
-        copy = remote(
-            pair_send.at[g], pair_recv.at[g], pair_ss.at[g], pair_rs.at[g], {"tp": tp_at(1)}
-        )
-        copy.start()
-        pairs.append(copy)
-        sent.append(copy)
+        remote(
+            pair_send.at[g], pair_recv.at[g], pair_ss, pair_rs.at[g], {"tp": tp_at(1)}
+        ).start()
         own_part[g] = outward(core)
     finish_pair(SEQ_GROUPS - 1)
 
@@ -425,32 +402,26 @@
                 :, pl.ds(pl.multiple_of(t * slice_w, slice_w), slice_w)
             ].T
 
-    mixes = []
     for g in range(SEQ_GROUPS):
         if g < 2:
             loads[4 + g].wait()
             transposed(*((wg, wg_t), (wu, wu_t))[g])
         total = stream_half[g * sg : (g + 1) * sg] + zs_send[g].astype(F32)
+        wait_all(zs_recv.at[g, pl.ds(1, levels - 1)], zs_rs.at[g])
         for d in range(1, levels):
-            zsum[g][-d].wait_recv()
             total = total + zs_recv[g, d].astype(F32)
         mix[core, my_ep, g] = total.astype(BF16)
         here = mix.at[core, my_ep, g]
-        step = []
         for k in reversed(range(n_ep)):
             for c in range(2):
                 if k or c:
-                    copy = remote(
+                    remote(
                         here,
                         here,
-                        mix_ss.at[g, k, c],
-                        mix_rs.at[g, k, c],
+                        mix_ss.at[c],
+                        mix_rs.at[c],
                         {"ep": ep_at(k), "tp": tp_at(c)},
-                    )
-                    copy.start()
-                    step.append(copy)
-        mixes += step
-    sent += mixes
+                    ).start()
 
     share = jnp.sum(
         jnp.where(routes[...] == my_ep, route_weights[...], 0.0), axis=0, keepdims=True
@@ -461,8 +432,8 @@
     )
     coefficient = jnp.sum(jnp.where(diagonal, share, 0.0), axis=1, keepdims=True)
     loads[6].wait()
-    for copy in mixes:
-        copy.wait_recv()
+    wait_all(mix.at[0, others], mix_rs.at[0])
+    wait_all(mix.at[1], mix_rs.at[1])
     halves = [mix[c].astype(F32).reshape(tokens, half_w) for c in range(2)]
     squares = sum(jnp.sum(half * half, axis=1, keepdims=True) for half in halves)
     inverse = lax.rsqrt(squares / width + 1e-06)
@@ -487,53 +458,53 @@
     up = matmul(normed_ffn, wu_t[...])
     hidden = (gate / (1.0 + jnp.exp(-gate)) * up).astype(BF16)
 
-    down = []
-    size = n_tp // DOWN_GROUPS
-    for g in reversed(range(DOWN_GROUPS)):
-        for d in reversed(range(g * size, (g + 1) * size)):
-            at = pl.ds(pl.multiple_of(tp_at(d) * slice_w, slice_w), slice_w)
-            product = (matmul(hidden, wd[:, at]) * coefficient).astype(BF16)
-            for e in range(n_ep):
-                dn_send[e, d] = product[e * seqs : (e + 1) * seqs]
-        step = []
-        group = pl.ds(g * size, size)
-        for k in reversed(range(1, n_ep)):
-            copy = remote(
-                dn_send.at[ep_at(k), group],
-                dn_recv.at[k, group],
-                dn_ss.at[g, k],
-                dn_rs.at[g, k],
-                {"ep": ep_at(k)},
-            )
-            copy.start()
-            step.append(copy)
-        down.append(step)
-        sent += step
-    final = []
-    for d in reversed(range(n_tp)):
-        if d % size == size - 1:
-            for copy in down[DOWN_GROUPS - 1 - d // size]:
-                copy.wait_recv()
-        summed = dn_send[my_ep, d].astype(F32)
-        for k in range(1, n_ep):
-            summed = summed + dn_recv[k, d].astype(F32)
-        if d:
-            fs_send[d] = summed.astype(BF16)
-            copy = remote(fs_send.at[d], fs_recv.at[d], fs_ss.at[d], fs_rs.at[d], {"tp": tp_at(d)})
-            copy.start()
-            final.append(copy)
-    sent += final
-    combined = summed
+    def downward(c, d):
+        at = (2 * flip(level, d) + c) * slice_w
+        return matmul(hidden, wd[:, pl.ds(pl.multiple_of(at, slice_w), slice_w)]) * coefficient
+
+    for d in reversed(range(levels)):
+        dpair_send[d] = downward(1 - core, d).astype(BF16)
+        remote(
+            dpair_send.at[d], dpair_recv.at[d], dpair_ss, dpair_rs.at[d], {"tp": tp_at(1)}
+        ).start()
+    for d in range(levels):
+        down_part[d] = downward(core, d)
+    for d in reversed(range(levels)):
+        wait_all(dpair_recv.at[d], dpair_rs.at[d])
+        summed = down_part[d] + dpair_recv[d].astype(F32)
+        for e in range(n_ep):
+            fs_send[d, e] = summed[e * seqs : (e + 1) * seqs].astype(BF16)
+        near = min(1, d)
+        for k in reversed(range(n_ep)):
+            if d or k:
+                remote(
+                    fs_send.at[d, ep_at(k)],
+                    fs_recv.at[d, k],
+                    fs_ss.at[near],
+                    fs_rs.at[near],
+                    {"ep": ep_at(k), "tp": tp_at(2 * d)},
+                ).start()
     own_stream = mix[
         core, my_ep, :, :, pl.ds(pl.multiple_of(level * slice_w, slice_w), slice_w)
     ].astype(F32).reshape(seqs, slice_w)
-    combined = own_stream + combined
-    for d in range(1, n_tp):
-        final[-d].wait_recv()
-        combined = combined + fs_recv[d].astype(F32)
+    combined = own_stream + fs_send[0, my_ep].astype(F32)
+    far = pl.ds(1, levels - 1)
+    wait_all(fs_recv.at[far], fs_rs.at[1])
+    wait_all(fs_recv.at[0, others], fs_rs.at[0])
+    for d in range(levels):
+        for k in range(n_ep):
+            if d or k:
+                combined = combined + fs_recv[d, k].astype(F32)
     out[...] = combined.astype(BF16)
-    for copy in sent:
-        copy.wait_send()
+    wait_all(a2a_send.at[others], a2a_ss)
+    wait_all(part_recv.at[:, others], part_ss)
+    wait_all(pair_send, pair_ss)
+    wait_all(zs_recv.at[:, far], zs_ss)
+    wait_all(mix.at[0, others], mix_ss.at[0])
+    wait_all(mix.at[1], mix_ss.at[1])
+    wait_all(dpair_send, dpair_ss)
+    wait_all(fs_recv.at[far], fs_ss.at[1])
+    wait_all(fs_recv.at[0, others], fs_ss.at[0])
 
 
 def shards(
@@ -611,43 +582,50 @@
             pltpu.VMEM((SEQ_GROUPS, sg, half_w), BF16),
             pltpu.VMEM((SEQ_GROUPS, levels, sg, half_w), BF16),
             pltpu.VMEM((2, n_ep, SEQ_GROUPS, sg, half_w), BF16),
-            pltpu.VMEM((n_ep, n_tp, seqs, slice_w), BF16),
-            pltpu.VMEM((n_ep, n_tp, seqs, slice_w), BF16),
-            pltpu.VMEM((n_tp, seqs, slice_w), BF16),
-            pltpu.VMEM((n_tp, seqs, slice_w), BF16),
+            pltpu.VMEM((levels, n_ep * seqs, slice_w), BF16),
+            pltpu.VMEM((levels, n_ep * seqs, slice_w), BF16),
+            pltpu.VMEM((levels, n_ep * seqs, slice_w), F32),
+            pltpu.VMEM((levels, n_ep, seqs, slice_w), BF16),
+            pltpu.VMEM((levels, n_ep, seqs, slice_w), BF16),
             dma((len(small),)),
             dma((7,)),
             dma((CACHE_LOADS,)),
             dma((CACHE_LOADS,)),
-            dma((n_ep,)),
-            dma((n_ep,)),
-            dma((3, n_ep)),
-            dma((3, n_ep)),
+            pltpu.SemaphoreType.REGULAR((max(1, levels.bit_length() - 2),)),
+            dma,
+            dma,
+            dma,
+            dma((3,)),
+            dma,
             dma((SEQ_GROUPS,)),
+            dma,
             dma((SEQ_GROUPS,)),
-            dma((SEQ_GROUPS, levels)),
-            dma((SEQ_GROUPS, levels)),
-            dma((SEQ_GROUPS, n_ep, 2)),
-            dma((SEQ_GROUPS, n_ep, 2)),
-            dma((DOWN_GROUPS, n_ep)),
-            dma((DOWN_GROUPS, n_ep)),
-            dma((n_tp,)),
-            dma((n_tp,)),
+            dma((2,)),
+            dma((2,)),
+            dma,
+            dma((levels,)),
+            dma((2,)),
+            dma((2,)),
         ],
         compiler_params=pltpu.CompilerParams(
-            collective_id=0, has_side_effects=True, vmem_limit_bytes=56 * 1024 * 1024
+            collective_id=0, has_side_effects=True, vmem_limit_bytes=48 * 1024 * 1024
         ),
     )(
-        *small,
-        w_query,
-        w_key,
-        w_value,
-        key_cache,
-        value_cache,
-        w_output,
-        jnp.swapaxes(w_expert_gate, 1, 2),
-        jnp.swapaxes(w_expert_up, 1, 2),
-        expert_down_weight,
+        *(
+            pltpu.with_memory_space_constraint(array, pltpu.HBM)
+            for array in (
+                *small,
+                w_query,
+                w_key,
+                w_value,
+                key_cache,
+                value_cache,
+                w_output,
+                jnp.swapaxes(w_expert_gate, 1, 2),
+                jnp.swapaxes(w_expert_up, 1, 2),
+                expert_down_weight,
+            )
+        )
     )
 
 

time: 37 us -> 32.9 us (0.89)
  Pallas kernels: 35.5 us -> 32.2 us
  local copies, waits for them, and re-layouts: 1.3 us -> 0.6 us
    pallas_call x1, Pallas kernels: 35.5 us -> 32.2 us  [shards(): pl.pallas_call(functools.partial(layer_kernel, n_ep, n_tp, heads), out_sh...]
    unnamed x1, local copies, waits for them, and re-layouts: 1.3 us -> 0.6 us
where the time goes in v2:
time: 32.9 us; the launch traced here: 32.8 us
  Pallas kernels  32.2 us (98%)
  local copies, waits for them, and re-layouts  0.6 us (2%)
    pallas_call x1, Pallas kernels, shards(): pl.pallas_call(functools.partial(layer_kernel, n_ep, n_tp, heads), out_sh...  32.2 us

profile of v2, /device:TPU:0, one launch (start us, length us, event | category | flops | bytes accessed | tf_op | source)
XLA Modules:
  0.0 32.8 jit_solution(12099342741065869158)
XLA Ops:
  0.0 32.2 %shard_map.172 = bf16[16,256]{1,0:T(8,128)(2,1)S(1)} custom-call(bf16[16,2048]{1,0:T(8,128)(2,1)} %stream_hbm.1, f32[1,2048]{1,0:T(1,128)} %bitcast.12, bf16[16,2048]{1,0:T(8,128)(2,1)} %bitcast.11, f32[1,16]{1,0:T(1,128)} %bitcast.16, f32[16,2,1024]{2,1,0:T(2,128)} %gates_hbm.1, s32[1,16]{1,0:T(1,128)} %bitcast.17, f32[1,2048]{1,0:T(1,128)} %bitcast.13, ...), custom_call_target="tpu_custom_call" | custom-call | tf_op jit(solution)/shard_map/pallas_call | solution.py:557
  32.2 0.6 %copy.20 = bf16[16,256]{1,0:T(8,128)(2,1)} copy(bf16[16,256]{1,0:T(8,128)(2,1)S(1)} %shard_map.172) | data formatting | bytes 16384

commit v3 on v2

--- a/solution.py
+++ b/solution.py
@@ -87,6 +87,8 @@
     own_part,
     zs_send,
     zs_recv,
+    zfar_send,
+    zfar_recv,
     mix,
     dpair_send,
     dpair_recv,
@@ -106,6 +108,8 @@
     pair_rs,
     zs_ss,
     zs_rs,
+    zfar_ss,
+    zfar_rs,
     mix_ss,
     mix_rs,
     dpair_ss,
@@ -202,7 +206,7 @@
     ]
     for load in small[:2] + loads[:3] + small[2:]:
         load.start()
-    for load in key_loads + value_loads + loads[3:]:
+    for load in key_loads:
         load.start(priority=1)
 
     spare = wg.shape[0] - hidden_w
@@ -222,6 +226,8 @@
     for k in reversed(range(1, n_ep)):
         remote(a2a_send.at[ep_at(k)], a2a_recv.at[k], a2a_ss, a2a_rs, {"ep": ep_at(k)}).start()
     a2a_recv[0] = a2a_send[my_ep]
+    for load in value_loads:
+        load.start(priority=1)
     for i, b in enumerate(bits[:-1]):
         pl.semaphore_signal(
             relay.at[i],
@@ -230,6 +236,13 @@
             device_id_type=pl.DeviceIdType.MESH,
         )
         pl.semaphore_wait(relay.at[i], 1)
+    pl.semaphore_signal(
+        relay.at[len(bits) - 1],
+        inc=1,
+        device_id={"tp": tp_at(1)},
+        device_id_type=pl.DeviceIdType.MESH,
+    )
+    pl.semaphore_wait(relay.at[len(bits) - 1], 1)
 
     for load in small[2:]:
         load.wait()
@@ -271,6 +284,13 @@
         position < live_count, forget_new + (last_gate - gate_rows[...]), -1e30
     )
 
+    for i in range(CACHE_LOADS // 2):
+        key_loads[i].wait()
+
+        @pl.loop(i * span, (i + 1) * span)
+        def _(s):
+            keys_t[pl.ds(pl.multiple_of(s * cols, cols), cols), :] = keys[s].T
+
     for load in loads[:3]:
         load.wait()
     wait_all(a2a_recv.at[others], a2a_rs)
@@ -284,7 +304,10 @@
             ).start()
         part_recv[i, 0] = product[:seqs]
 
-    for i in range(CACHE_LOADS):
+    for load in loads[3:]:
+        load.start(priority=1)
+
+    for i in range(CACHE_LOADS // 2, CACHE_LOADS):
         key_loads[i].wait()
 
         @pl.loop(i * span, (i + 1) * span)
@@ -317,16 +340,12 @@
     def finish_pair(g):
         wait_all(pair_recv.at[g], pair_rs.at[g])
         zs_send[g] = (own_part[g] + pair_recv[g].astype(F32)).astype(BF16)
-        for d in reversed(range(1, levels)):
+        for d in reversed(range(1, levels - 1)):
             remote(
                 zs_send.at[g], zs_recv.at[g, d], zs_ss, zs_rs.at[g], {"tp": tp_at(2 * d)}
             ).start()
 
-    for g in range(SEQ_GROUPS):
-        found = score(g)
-        if g == 0:
-            key_new = projected(1)
-            value_new = projected(2)
+    def soften(g, found):
         mine = slice(g * sg, (g + 1) * sg)
         own_score = (
             by_head(
@@ -346,13 +365,22 @@
         past = jnp.exp(full - largest)
         own_term = jnp.exp(own_score - largest)
         total = jnp.sum(past, axis=1, keepdims=True) + own_term
-        past_weights = past / total
-        own_weight = (own_term / total).astype(BF16).astype(F32)
-        if g:
-            finish_pair(g - 1)
-        for i in range(CACHE_LOADS):
-            if i * span // sg == g:
-                value_loads[i].wait()
+        return past / total, (own_term / total).astype(BF16).astype(F32)
+
+    found = score(0)
+    key_new = projected(1)
+    value_new = projected(2)
+    for load in value_loads:
+        load.wait()
+    loads[3].wait()
+    softened = []
+    for g in range(SEQ_GROUPS):
+        later = score(g + 1) if g + 1 < SEQ_GROUPS else None
+        softened.append(soften(g, found))
+        found = later
+    for g in range(SEQ_GROUPS):
+        mine = slice(g * sg, (g + 1) * sg)
+        past_weights, own_weight = softened[g]
         gathered = jnp.zeros((grows, cols), F32)
         for s in range(sg):
             chosen = jnp.where(group_seq == s, past_weights, 0.0).astype(BF16)
@@ -364,8 +392,8 @@
                 lane_head == h, gathered[part] + own_weight[part] * value_new[mine], attended
             )
         attended = attended.astype(BF16)
-        if g == 0:
-            loads[3].wait()
+        if g:
+            finish_pair(g - 1)
 
         def outward(c):
             return jnp.concatenate(
@@ -380,11 +408,32 @@
             )
 
         pair_send[g] = outward(1 - core).astype(BF16)
+        last = 2 * (levels - 1)
+        remote(
+            pair_send.at[g], zfar_recv.at[g, 1], zfar_ss, zfar_rs.at[g], {"tp": tp_at(last + 1)}
+        ).start()
         remote(
             pair_send.at[g], pair_recv.at[g], pair_ss, pair_rs.at[g], {"tp": tp_at(1)}
         ).start()
         own_part[g] = outward(core)
+        zfar_send[g] = own_part[g].astype(BF16)
+        remote(
+            zfar_send.at[g], zfar_recv.at[g, 0], zfar_ss, zfar_rs.at[g], {"tp": tp_at(last)}
+        ).start()
+    def transposed(src, dst, low, high):
+        @pl.loop(low, high)
+        def _(t):
+            into = lax.rem(t, 2) * half_w + lax.div(t, 2) * slice_w
+            dst[pl.ds(pl.multiple_of(into, slice_w), slice_w), :] = src[
+                :, pl.ds(pl.multiple_of(t * slice_w, slice_w), slice_w)
+            ].T
+
+    loads[4].wait()
+    loads[5].wait()
+    transposed(wg, wg_t, 0, n_tp // 2)
     finish_pair(SEQ_GROUPS - 1)
+    transposed(wg, wg_t, n_tp // 2, n_tp)
+    transposed(wu, wu_t, 0, n_tp)
 
     stream_half = jnp.concatenate(
         [
@@ -394,22 +443,13 @@
         axis=1,
     ).astype(F32)
 
-    def transposed(src, dst):
-        @pl.loop(0, n_tp)
-        def _(t):
-            into = lax.rem(t, 2) * half_w + lax.div(t, 2) * slice_w
-            dst[pl.ds(pl.multiple_of(into, slice_w), slice_w), :] = src[
-                :, pl.ds(pl.multiple_of(t * slice_w, slice_w), slice_w)
-            ].T
-
     for g in range(SEQ_GROUPS):
-        if g < 2:
-            loads[4 + g].wait()
-            transposed(*((wg, wg_t), (wu, wu_t))[g])
         total = stream_half[g * sg : (g + 1) * sg] + zs_send[g].astype(F32)
-        wait_all(zs_recv.at[g, pl.ds(1, levels - 1)], zs_rs.at[g])
-        for d in range(1, levels):
+        wait_all(zs_recv.at[g, pl.ds(1, levels - 2)], zs_rs.at[g])
+        for d in range(1, levels - 1):
             total = total + zs_recv[g, d].astype(F32)
+        wait_all(zfar_recv.at[g], zfar_rs.at[g])
+        total = total + zfar_recv[g, 0].astype(F32) + zfar_recv[g, 1].astype(F32)
         mix[core, my_ep, g] = total.astype(BF16)
         here = mix.at[core, my_ep, g]
         for k in reversed(range(n_ep)):
@@ -499,7 +539,8 @@
     wait_all(a2a_send.at[others], a2a_ss)
     wait_all(part_recv.at[:, others], part_ss)
     wait_all(pair_send, pair_ss)
-    wait_all(zs_recv.at[:, far], zs_ss)
+    wait_all(zs_recv.at[:, pl.ds(1, levels - 2)], zs_ss)
+    wait_all(zfar_recv, zfar_ss)
     wait_all(mix.at[0, others], mix_ss.at[0])
     wait_all(mix.at[1], mix_ss.at[1])
     wait_all(dpair_send, dpair_ss)
@@ -581,6 +622,8 @@
             pltpu.VMEM((SEQ_GROUPS, sg, half_w), F32),
             pltpu.VMEM((SEQ_GROUPS, sg, half_w), BF16),
             pltpu.VMEM((SEQ_GROUPS, levels, sg, half_w), BF16),
+            pltpu.VMEM((SEQ_GROUPS, sg, half_w), BF16),
+            pltpu.VMEM((SEQ_GROUPS, 2, sg, half_w), BF16),
             pltpu.VMEM((2, n_ep, SEQ_GROUPS, sg, half_w), BF16),
             pltpu.VMEM((levels, n_ep * seqs, slice_w), BF16),
             pltpu.VMEM((levels, n_ep * seqs, slice_w), BF16),
@@ -591,11 +634,13 @@
             dma((7,)),
             dma((CACHE_LOADS,)),
             dma((CACHE_LOADS,)),
-            pltpu.SemaphoreType.REGULAR((max(1, levels.bit_length() - 2),)),
+            pltpu.SemaphoreType.REGULAR((levels.bit_length() - 1,)),
             dma,
             dma,
             dma,
             dma((3,)),
+            dma,
+            dma((SEQ_GROUPS,)),
             dma,
             dma((SEQ_GROUPS,)),
             dma,

time: 32.9 us -> 32.9 us (level)
  no operation moved by 1% of the time
where the time goes in v3:
time: 32.9 us; the launch traced here: 32.8 us
  Pallas kernels  32.2 us (98%)
  local copies, waits for them, and re-layouts  0.6 us (2%)
    pallas_call x1, Pallas kernels, shards(): pl.pallas_call(functools.partial(layer_kernel, n_ep, n_tp, heads), out_sh...  32.2 us

profile of v3, /device:TPU:0, one launch (start us, length us, event | category | flops | bytes accessed | tf_op | source)
XLA Modules:
  0.0 32.8 jit_solution(8265663413994530052)
XLA Ops:
  0.0 32.2 %shard_map.172 = bf16[16,256]{1,0:T(8,128)(2,1)S(1)} custom-call(bf16[16,2048]{1,0:T(8,128)(2,1)} %stream_hbm.1, f32[1,2048]{1,0:T(1,128)} %bitcast.12, bf16[16,2048]{1,0:T(8,128)(2,1)} %bitcast.11, f32[1,16]{1,0:T(1,128)} %bitcast.16, f32[16,2,1024]{2,1,0:T(2,128)} %gates_hbm.1, s32[1,16]{1,0:T(1,128)} %bitcast.17, f32[1,2048]{1,0:T(1,128)} %bitcast.13, ...), custom_call_target="tpu_custom_call" | custom-call | tf_op jit(solution)/shard_map/pallas_call | solution.py:598
  32.2 0.6 %copy.20 = bf16[16,256]{1,0:T(8,128)(2,1)} copy(bf16[16,256]{1,0:T(8,128)(2,1)S(1)} %shard_map.172) | data formatting | bytes 16384

commit v4 on v3

--- a/solution.py
+++ b/solution.py
@@ -228,21 +228,16 @@
     a2a_recv[0] = a2a_send[my_ep]
     for load in value_loads:
         load.start(priority=1)
-    for i, b in enumerate(bits[:-1]):
+
+    def tell(i, d):
         pl.semaphore_signal(
             relay.at[i],
             inc=1,
-            device_id={"tp": tp_at(2 * b)},
+            device_id={"tp": tp_at(d)},
             device_id_type=pl.DeviceIdType.MESH,
         )
-        pl.semaphore_wait(relay.at[i], 1)
-    pl.semaphore_signal(
-        relay.at[len(bits) - 1],
-        inc=1,
-        device_id={"tp": tp_at(1)},
-        device_id_type=pl.DeviceIdType.MESH,
-    )
-    pl.semaphore_wait(relay.at[len(bits) - 1], 1)
+
+    tell(0, 2 * bits[0])
 
     for load in small[2:]:
         load.wait()
@@ -307,6 +302,10 @@
     for load in loads[3:]:
         load.start(priority=1)
 
+    for i in range(len(bits) - 1):
+        pl.semaphore_wait(relay.at[i], 1)
+        tell(i + 1, 2 * bits[i + 1] if i + 2 < len(bits) else 1)
+
     for i in range(CACHE_LOADS // 2, CACHE_LOADS):
         key_loads[i].wait()
 
@@ -368,6 +367,7 @@
         return past / total, (own_term / total).astype(BF16).astype(F32)
 
     found = score(0)
+    pl.semaphore_wait(relay.at[len(bits) - 1], 1)
     key_new = projected(1)
     value_new = projected(2)
     for load in value_loads:

time: 32.9 us -> 32.3 us (0.982)
  Pallas kernels: 32.2 us -> 31.6 us
    pallas_call x1, Pallas kernels: 32.2 us -> 31.6 us  [shards(): pl.pallas_call(functools.partial(layer_kernel, n_ep, n_tp, heads), out_sh...]
where the time goes in v4:
time: 32.3 us; the launch traced here: 32.2 us
  Pallas kernels  31.6 us (98%)
  local copies, waits for them, and re-layouts  0.6 us (2%)
    pallas_call x1, Pallas kernels, shards(): pl.pallas_call(functools.partial(layer_kernel, n_ep, n_tp, heads), out_sh...  31.6 us

profile of v4, /device:TPU:0, one launch (start us, length us, event | category | flops | bytes accessed | tf_op | source)
XLA Modules:
  0.0 32.2 jit_solution(18251551291000422711)
XLA Ops:
  0.0 31.6 %shard_map.172 = bf16[16,256]{1,0:T(8,128)(2,1)S(1)} custom-call(bf16[16,2048]{1,0:T(8,128)(2,1)} %stream_hbm.1, f32[1,2048]{1,0:T(1,128)} %bitcast.12, bf16[16,2048]{1,0:T(8,128)(2,1)} %bitcast.11, f32[1,16]{1,0:T(1,128)} %bitcast.16, f32[16,2,1024]{2,1,0:T(2,128)} %gates_hbm.1, s32[1,16]{1,0:T(1,128)} %bitcast.17, f32[1,2048]{1,0:T(1,128)} %bitcast.13, ...), custom_call_target="tpu_custom_call" | custom-call | tf_op jit(solution)/shard_map/pallas_call | solution.py:598
  31.6 0.6 %copy.20 = bf16[16,256]{1,0:T(8,128)(2,1)} copy(bf16[16,256]{1,0:T(8,128)(2,1)S(1)} %shard_map.172) | data formatting | bytes 16384
